TPU v7x, 32 devices: a whole 2x2x4 slice. The times are simulated.
32 devices in a mesh: ep: 8 (over z, y), tp: 4 (over x, core).
Axes of the slice: x: 2, y: 2, z: 4, core: 2. Of those that a mesh axis runs over, the one named last changes fastest.
Arguments:
- tokens: bfloat16 [192, 2048], P('ep'), may hold values from -6 to 6
- delta_state: float32 [192, 8, 128, 128], P('ep', 'tp'), may hold values from -3 to 3
- first_gain: bfloat16 [2048], replicated, may hold values from 0.099609375 to 1.8984375
- query_weight: bfloat16 [2048, 1024], P(None, 'tp'), may hold values from -0.125 to 0.125
- key_weight: bfloat16 [2048, 1024], P(None, 'tp'), may hold values from -0.125 to 0.125
- value_weight: bfloat16 [2048, 1024], P(None, 'tp'), may hold values from -0.125 to 0.125
- outgate_weight: bfloat16 [2048, 1024], P(None, 'tp'), may hold values from -0.125 to 0.125
- beta_weight: bfloat16 [2048, 8], replicated, may hold values from -0.125 to 0.125
- decay_weight: bfloat16 [2048, 8], replicated, may hold values from -0.125 to 0.125
- decay_rate: float32 [8], replicated, may hold values from 0.05 to 4
- decay_bias: float32 [8], replicated, may hold values from -3 to 3
- head_gain: bfloat16 [128], replicated, may hold values from 0.099609375 to 1.8984375
- out_weight: bfloat16 [1024, 2048], P('tp'), may hold values from -0.1875 to 0.1875
- second_gain: bfloat16 [2048], replicated, may hold values from 0.099609375 to 1.8984375
- blend_weight: bfloat16 [2048], replicated, may hold values from -0.125 to 0.125
- dense_gate_weight: bfloat16 [2048, 2048], P(None, 'tp'), may hold values from -0.125 to 0.125
- dense_up_weight: bfloat16 [2048, 2048], P(None, 'tp'), may hold values from -0.125 to 0.125
- dense_down_weight: bfloat16 [2048, 2048], P('tp'), may hold values from -0.125 to 0.125
- expert_gate: bfloat16 [32, 2048, 512], P(('ep', 'tp')), may hold values from -0.125 to 0.125
- expert_up: bfloat16 [32, 2048, 512], P(('ep', 'tp')), may hold values from -0.125 to 0.125
- expert_down: bfloat16 [32, 512, 2048], P(('ep', 'tp')), may hold values from -0.25 to 0.25
- route_ids: int32 [192, 6], P('ep'), may hold values from 0 to 31, all different within a row; in each aligned block of 24 rows (0 to 23, 24 to 47, ...) at most 7 rows name the same one
- route_weights: float32 [192, 6], P('ep'), may hold values from 0.1 to 1
Outputs:
- new_tokens: bfloat16 [192, 2048], P('ep')
- new_state: float32 [192, 8, 128, 128], P('ep', 'tp')
Inputs may be any that keep to these rules, and one draw needn't show every extreme that they name: `route_ids`: each row names 6 different experts. In each aligned block of 24 rows (the sequences of one index of ep) no expert is named by more than 7 rows, and in some block an expert is named by exactly 7 rows.
All inputs are finite; a program needn't handle non-finite values.
Results may differ from a plain program's by a relative error of at most 0.017.
Values may be sent and summed in bfloat16 or wider, within the bound.
A program may use at most 128 MiB of HBM per device.

v0:
```python
import jax
import jax.numpy as jnp
from jax import lax
from jax.sharding import PartitionSpec as P

norm_eps = 1e-06
unit_eps = 1e-06
routed_scale = 2.5


def rms_scale(values, gain):
    values = values.astype(jnp.float32)
    inverse = lax.rsqrt(jnp.mean(values * values, axis=-1, keepdims=True) + norm_eps)
    return values * inverse * gain.astype(jnp.float32)


def unit_rows(values):
    return values * lax.rsqrt(jnp.sum(values * values, axis=-1, keepdims=True) + unit_eps)


def rounded(values):
    return lax.optimization_barrier(values.astype(jnp.bfloat16)).astype(jnp.float32)


def delta_update(delta_state, query_raw, key_raw, value_raw, beta_gate, log_decay):
    head_size = delta_state.shape[-1]
    query_unit = unit_rows(jax.nn.silu(query_raw)) * head_size ** (-0.5)
    key_unit = unit_rows(jax.nn.silu(key_raw))
    value_act = jax.nn.silu(value_raw)
    decayed = jnp.exp(log_decay)[:, :, None, None] * delta_state
    predicted = jnp.einsum("shkv,shk->shv", decayed, key_unit, precision=lax.Precision.HIGHEST)
    update = (beta_gate[:, :, None] * key_unit)[:, :, :, None] * (value_act - predicted)[
        :, :, None, :
    ]
    new_state = decayed + update
    readout = jnp.einsum("shkv,shk->shv", new_state, query_unit, precision=lax.Precision.HIGHEST)
    return (new_state, readout)


def gated_heads(readout, outgate_raw, head_gain):
    scaled = rms_scale(readout, head_gain) * jax.nn.silu(outgate_raw)
    return scaled.reshape(scaled.shape[0], -1).astype(jnp.bfloat16)


def expert_rows(row_block, gate_mat, up_mat, down_mat):
    gate_part = jnp.dot(row_block, gate_mat, preferred_element_type=jnp.float32)
    up_part = jnp.dot(row_block, up_mat, preferred_element_type=jnp.float32)
    hidden = (jax.nn.silu(gate_part) * up_part).astype(jnp.bfloat16)
    return jnp.dot(hidden, down_mat, preferred_element_type=jnp.float32).astype(jnp.bfloat16)


def shards(
    tokens,
    delta_state,
    first_gain,
    query_weight,
    key_weight,
    value_weight,
    outgate_weight,
    beta_weight,
    decay_weight,
    decay_rate,
    decay_bias,
    head_gain,
    out_weight,
    second_gain,
    blend_weight,
    dense_gate_weight,
    dense_up_weight,
    dense_down_weight,
    expert_gate,
    expert_up,
    expert_down,
    route_ids,
    route_weights,
):
    seq_count = tokens.shape[0]
    head_local = delta_state.shape[1]
    head_size = delta_state.shape[2]
    top_count = route_ids.shape[1]
    ep_count = lax.axis_size("ep")
    tp_count = lax.axis_size("tp")
    tp_index = lax.axis_index("tp")
    normed = rms_scale(tokens, first_gain).astype(jnp.bfloat16)

    def project(weight):
        product = jnp.dot(normed, weight, preferred_element_type=jnp.float32)
        return rounded(product).reshape(seq_count, head_local, head_size)

    query_raw = project(query_weight)
    key_raw = project(key_weight)
    value_raw = project(value_weight)
    outgate_raw = project(outgate_weight)
    head_start = tp_index * head_local
    beta_all = jax.nn.sigmoid(jnp.dot(normed, beta_weight, preferred_element_type=jnp.float32))
    beta_gate = lax.dynamic_slice_in_dim(beta_all, head_start, head_local, 1)
    decay_input = jnp.dot(normed, decay_weight, preferred_element_type=jnp.float32) + decay_bias
    decay_all = -decay_rate * jax.nn.softplus(decay_input)
    log_decay = lax.dynamic_slice_in_dim(decay_all, head_start, head_local, 1)
    new_state, readout = delta_update(
        delta_state, query_raw, key_raw, value_raw, beta_gate, log_decay
    )
    gated = gated_heads(readout, outgate_raw, head_gain)
    mix_part = jnp.dot(gated, out_weight, preferred_element_type=jnp.float32)
    row_local = seq_count // tp_count
    mixed_rows = lax.psum_scatter(
        mix_part.astype(jnp.bfloat16), "tp", scatter_dimension=0, tiled=True
    ).astype(jnp.float32)
    own_tokens = lax.dynamic_slice_in_dim(tokens, tp_index * row_local, row_local, 0)
    residual_rows = (own_tokens.astype(jnp.float32) + mixed_rows).astype(jnp.bfloat16)
    normed_rows = rms_scale(residual_rows, second_gain).astype(jnp.bfloat16)
    normed_mid, residual = (
        lax.all_gather(normed_rows, "tp", axis=0, tiled=True),
        lax.all_gather(residual_rows, "tp", axis=0, tiled=True),
    )
    blend_gate = jax.nn.sigmoid(
        jnp.dot(normed_mid, blend_weight, preferred_element_type=jnp.float32)
    )
    dense_gate_raw = jnp.dot(normed_mid, dense_gate_weight, preferred_element_type=jnp.float32)
    dense_up_raw = jnp.dot(normed_mid, dense_up_weight, preferred_element_type=jnp.float32)
    dense_hidden = (jax.nn.silu(dense_gate_raw) * dense_up_raw).astype(jnp.bfloat16)
    dense_part = jnp.dot(dense_hidden, dense_down_weight, preferred_element_type=jnp.float32)
    expert_count = ep_count * tp_count
    capacity = max(2, (3 * seq_count * top_count + 2 * expert_count - 1) // (2 * expert_count))
    flat_ids = route_ids.reshape(-1)
    assign_count = flat_ids.shape[0]
    earlier = jnp.arange(assign_count)[:, None] > jnp.arange(assign_count)[None, :]
    matches = (flat_ids[:, None] == flat_ids[None, :]) & earlier
    rank_of = jnp.sum(matches.astype(jnp.int32), axis=1)
    owned = flat_ids % tp_count == tp_index
    slot_of = jnp.where(owned, flat_ids // tp_count * capacity + rank_of, -1)
    slot_total = ep_count * capacity
    slot_grid = slot_of.reshape(seq_count, top_count)
    slot_range = jnp.arange(slot_total, dtype=jnp.int32)
    dispatch = jnp.any(slot_grid[None, :, :] == slot_range[:, None, None], axis=2).astype(
        jnp.bfloat16
    )
    model_width = normed_mid.shape[1]
    outgoing = jnp.dot(dispatch, normed_mid, preferred_element_type=jnp.float32).astype(
        jnp.bfloat16
    )
    outgoing = outgoing.reshape(ep_count, capacity, model_width)
    arrived = lax.all_to_all(outgoing, "ep", split_axis=0, concat_axis=0, tiled=True)
    result = expert_rows(
        arrived.reshape(-1, model_width), expert_gate[0], expert_up[0], expert_down[0]
    )
    returned = lax.all_to_all(
        result.reshape(arrived.shape), "ep", split_axis=0, concat_axis=0, tiled=True
    )
    returned_rows = returned.reshape(slot_total, model_width)
    picked = returned_rows[jnp.maximum(slot_of, 0)].astype(jnp.float32)
    picked = picked.reshape(seq_count, top_count, model_width)
    route_scale = route_weights / jnp.sum(route_weights, axis=1, keepdims=True) * routed_scale
    kept_scale = jnp.where(owned.reshape(seq_count, top_count), route_scale, 0.0)
    routed_part = jnp.sum(kept_scale[:, :, None] * picked, axis=1)
    combined = lax.psum(
        (routed_part + blend_gate[:, None] * dense_part).astype(jnp.bfloat16), "tp"
    ).astype(jnp.float32)
    new_tokens = (residual.astype(jnp.float32) + combined).astype(jnp.bfloat16)
    return (new_tokens, new_state)


def solution(mesh):
    placed = (
        P("ep", None),
        P("ep", "tp", None, None),
        P(),
        P(None, "tp"),
        P(None, "tp"),
        P(None, "tp"),
        P(None, "tp"),
        P(),
        P(),
        P(),
        P(),
        P(),
        P("tp", None),
        P(),
        P(),
        P(None, "tp"),
        P(None, "tp"),
        P("tp", None),
        P(("ep", "tp"), None, None),
        P(("ep", "tp"), None, None),
        P(("ep", "tp"), None, None),
        P("ep", None),
        P("ep", None),
    )
    return jax.shard_map(
        shards,
        mesh=mesh,
        in_specs=placed,
        out_specs=(P("ep", None), P("ep", "tp", None, None)),
        check_vma=False,
    )
```

profile of v0, /device:TPU:0, one launch (start us, length us, event | category | flops | bytes accessed | tf_op | source)
XLA Modules:
  0.0 129.9 jit_solution(16252030878266203387)
XLA Ops:
  7.2 0.0 copy-start
  7.2 0.0 copy-start.3
  7.2 0.8 convert_element_type.92
  8.0 1.1 fusion.27
  9.1 0.7 neg.38
  9.8 1.1 fusion.22
  10.9 1.2 fusion.59
  12.1 0.1 copy.48
  12.2 1.6 %convolution_convert_fusion.6 = bf16[24,256]{1,0:T(8,128)(2,1)S(1)} fusion(bf16[2048,256]{1,0:T(8,128)(2,1)} %param.27, bf16[24,2048]{1,0:T(8,128)(2,1)} %param.23, f32[2048]{0:T(1024)S(1)} %convert_element_type.92, f32[24]{0:T(128)S(1)} %add_rsqrt_fusion.4), kind=kOutput, calls=%fused_computation.24 | convolution fusion | flops 25368576 | bytes 1167456 | tf_op jit(solution)/shard_map/dot_general | solution.py:87
  13.8 0.1 multiply_reduce_fusion.3
  13.9 0.1 copy.47
  14.0 1.6 %convolution_convert_fusion.5 = bf16[24,256]{1,0:T(8,128)(2,1)S(1)} fusion(bf16[2048,256]{1,0:T(8,128)(2,1)} %param.28, bf16[24,2048]{1,0:T(8,128)(2,1)} %param.23, f32[2048]{0:T(1024)S(1)} %convert_element_type.92, f32[24]{0:T(128)S(1)} %add_rsqrt_fusion.4), kind=kOutput, calls=%fused_computation.23 | convolution fusion | flops 25368576 | bytes 1167456 | tf_op jit(solution)/shard_map/dot_general | solution.py:87
  15.6 0.3 convolution_convert_fusion.4
  16.0 0.1 multiply_reduce_fusion.2
  16.1 0.1 broadcast_multiply_fusion.1
  16.2 4.9 %fusion.1 = f32[24,2,1,128]{3,2,1,0:T(1,128)S(1)} fusion(f32[24,2,128,1]{2,3,1,0:T(1,128)S(1)} %bitcast.71, f32[24,2,128,128]{3,2,1,0:T(8,128)} %param.24, f32[24,2]{1,0:T(8,128)S(1)} %copy.47), kind=kOutput, calls=%fused_computation.2 | convolution fusion | flops 10223616 | bytes 3195072 | tf_op jit(solution)/shard_map/shkv,shk->shv/dot_general | solution.py:31
  21.2 1.1 multiply_add_fusion
  22.3 0.0 copy-start.2
  22.4 0.1 multiply_multiply_fusion
  22.5 1.5 %copy-done.2 = f32[24,2,128,128]{3,2,1,0:T(8,128)} copy-done((f32[24,2,128,128]{3,2,1,0:T(8,128)}, f32[24,2,128,128]{3,2,1,0:T(8,128)S(1)}, u32[]{:S(2)}) %copy-start.2) | copy-done | bytes 3145752
  24.0 2.8 %fusion.69 = f32[24,2,1,128]{3,2,1,0:T(1,128)S(1)} fusion(f32[24,2,128,128]{3,2,1,0:T(8,128)S(1)} %multiply_add_fusion, f32[24,2,128,1]{2,3,1,0:T(1,128)S(1)} %bitcast.73), kind=kOutput, calls=%fused_computation.112 | convolution fusion | flops 9437184 | bytes 3194880 | tf_op jit(solution)/shard_map/shkv,shk->shv/dot_general | solution.py:36
  26.8 0.1 multiply_reduce_fusion.1
  26.9 0.3 convolution_convert_fusion.3
  27.2 0.0 copy-start.9
  27.3 0.1 fusion.50
  27.4 0.2 convolution_convert_fusion.2
  27.6 9.7 %fusion = bf16[8,2048]{1,0:T(8,128)(2,1)S(1)} fusion(bf16[24,2048]{1,0:T(8,128)(2,1)S(1)} %convolution_convert_fusion.2), kind=kCustom, calls=%all-reduce-scatter | all-reduce-scatter fusion | flops 65537 | bytes 131584
  37.3 1.3 collective-permute-start
  38.6 0.1 copy.49
  38.7 0.1 eq.52
  38.8 0.2 convert_reduce_fusion
  39.0 0.1 reduce_sum.82
  39.1 0.1 copy.55
  39.2 0.1 fusion.36
  39.3 0.1 reshape.273
  39.5 0.6 dynamic-slice.4
  40.7 0.2 concatenate
  40.9 0.2 fusion.37
  41.0 0.1 fusion.46
  41.1 7.0 %all-gather.1 = bf16[4,6,2048]{2,1,0:T(8,128)(2,1)S(1)} all-gather(bf16[1,6,2048]{2,1,0:T(8,128)(2,1)S(1)} %fusion.46), channel_id=1, replica_groups=mesh['ep'=8,'tp'=4] {'tp'}, dimensions={0}, use_global_device_ids=true | all-gather | bytes 122880 | tf_op jit(solution)/shard_map/all_gather | solution.py:113
  48.1 0.3 convolution_convert_fusion.1
  48.4 0.8 reshape.269
  49.2 5.8 %all-to-all-start = ((bf16[8,7,2048]{2,1,0:T(8,128)(2,1)}), bf16[8,7,2048]{2,1,0:T(8,128)(2,1)S(1)}, u32[]{:S(2)}, u32[]{:S(2)}) async-start(bf16[8,7,2048]{2,1,0:T(8,128)(2,1)} %reshape.269), calls=%async_computation | async-start | bytes 524288 | tf_op jit(solution)/shard_map/all_to_all | solution.py:143
  55.0 0.1 copy.52
  55.2 0.1 multiply_select_fusion
  55.2 9.2 %all-to-all-done = bf16[8,7,2048]{2,1,0:T(8,128)(2,1)S(1)} async-done(((bf16[8,7,2048]{2,1,0:T(8,128)(2,1)}), bf16[8,7,2048]{2,1,0:T(8,128)(2,1)S(1)}, u32[]{:S(2)}, u32[]{:S(2)}) %all-to-all-start) | async-done | bytes 229408 | tf_op jit(solution)/shard_map/all_to_all | solution.py:143
  64.4 0.1 reshape.270
  64.5 2.0 %fusion.8 = f32[56,512]{1,0:T(8,128)S(1)} fusion(bf16[56,2048]{1,0:T(8,128)(2,1)S(1)} %reshape.270, bf16[1,2048,512]{2,1,0:T(8,128)(2,1)} %param.41), kind=kOutput, calls=%fused_computation.13 | convolution fusion | flops 117440512 | bytes 2441216 | tf_op jit(solution)/shard_map/dot_general | solution.py:46
  66.6 2.5 %convolution_convert_fusion = bf16[56,2048]{1,0:T(8,128)(2,1)S(1)} fusion(bf16[1,512,2048]{2,1,0:T(8,128)(2,1)S(1)} %copy-done, bf16[56,2048]{1,0:T(8,128)(2,1)S(1)} %reshape.270, bf16[1,2048,512]{2,1,0:T(8,128)(2,1)} %param.42, f32[56,512]{1,0:T(8,128)S(1)} %fusion.8), kind=kOutput, calls=%fused_computation.4 | convolution fusion | flops 235167744 | bytes 4767744 | tf_op jit(solution)/shard_map/dot_general | solution.py:49
  69.1 0.8 reshape.271
  69.8 3.6 %all-to-all-start.1 = ((bf16[8,7,2048]{2,1,0:T(8,128)(2,1)}), bf16[8,7,2048]{2,1,0:T(8,128)(2,1)S(1)}, u32[]{:S(2)}, u32[]{:S(2)}) async-start(bf16[8,7,2048]{2,1,0:T(8,128)(2,1)} %reshape.271), calls=%async_computation.1 | async-start | bytes 524288 | tf_op jit(solution)/shard_map/all_to_all | solution.py:147
  73.4 0.2 all-reduce.4.cloned.1.call-start
  73.6 0.1 fusion.26
  73.8 2.0 %fusion.70 = f32[24,512]{1,0:T(8,128)S(1)} fusion(bf16[24,2048]{1,0:T(8,128)(2,1)S(1)} %reshape.294, bf16[2048,512]{1,0:T(8,128)(2,1)} %param.38), kind=kOutput, calls=%fused_computation.113 | convolution fusion | flops 50331648 | bytes 2244608 | tf_op jit(solution)/shard_map/dot_general | solution.py:119
  75.8 6.6 %all-to-all-done.1 = bf16[8,7,2048]{2,1,0:T(8,128)(2,1)S(1)} async-done(((bf16[8,7,2048]{2,1,0:T(8,128)(2,1)}), bf16[8,7,2048]{2,1,0:T(8,128)(2,1)S(1)}, u32[]{:S(2)}, u32[]{:S(2)}) %all-to-all-start.1) | async-done | bytes 229408 | tf_op jit(solution)/shard_map/all_to_all | solution.py:147
  82.4 0.1 reshape.272
  82.5 1.0 gather_fusion
  83.5 1.3 %reshape.282 = f32[24,6,2048]{2,1,0:T(8,128)} reshape(bf16[144,2048]{1,0:T(8,128)(2,1)S(1)} %gather_fusion) | data formatting | bytes 1769472 | tf_op jit(solution)/shard_map/convert_element_type | solution.py:151
  84.8 2.0 %multiply_reduce_fusion = f32[24,2048]{1,0:T(8,128)S(1)} fusion(f32[24,6,2048]{2,1,0:T(8,128)} %reshape.282, f32[24,6]{1,0:T(8,128)S(1)} %multiply_select_fusion), kind=kLoop, calls=%fused_computation.15 | loop fusion | flops 540672 | bytes 1376832 | tf_op jit(solution)/shard_map/reduce_sum | solution.py:155
  86.8 3.6 %fusion.4 = bf16[24,2048]{1,0:T(8,128)(2,1)} fusion(f32[24,2048]{1,0:T(8,128)S(1)} %multiply_reduce_fusion, bf16[512,2048]{1,0:T(8,128)(2,1)} %param.40, bf16[24,2048]{1,0:T(8,128)(2,1)S(1)} %reshape.294, bf16[2048,512]{1,0:T(8,128)(2,1)} %param.39, f32[24]{0:T(128)S(1)} %fusion.26, f32[24,512]{1,0:T(8,128)S(1)} %fusion.70), kind=kOutput, calls=%fused_computation.8 | convolution fusion | flops 100884480 | bytes 4636768 | tf_op jit(solution)/shard_map/dot_general | solution.py:122
  90.4 0.0 all-reduce.4.cloned.1.call-update
  90.4 5.4 %all-gather = bf16[4,6,2048]{2,1,0:T(8,128)(2,1)S(1)} all-gather(bf16[1,6,2048]{2,1,0:T(8,128)(2,1)S(1)} %bitcast.68), channel_id=1, replica_groups=mesh['ep'=8,'tp'=4] {'tp'}, dimensions={0}, use_global_device_ids=true | all-gather | bytes 122880 | tf_op jit(solution)/shard_map/all_gather | solution.py:114
  95.9 25.7 %all-reduce.4.cloned.1.call-done = bf16[24,2048]{1,0:T(8,128)(2,1)} async-done(((bf16[24,2048]{1,0:T(8,128)(2,1)}), bf16[24,2048]{1,0:T(8,128)(2,1)}) %all-reduce.4.cloned.1.call-update) | async-done | bytes 98320 | tf_op jit(solution)/shard_map/psum | solution.py:156
  121.5 1.6 %add_convert_fusion = bf16[24,2048]{1,0:T(8,128)(2,1)} fusion(f32[24,2048]{1,0:T(8,128)S(1)} %reshape.295, bf16[24,2048]{1,0:T(8,128)(2,1)} %all-reduce.4.cloned.1.call-done), kind=kLoop, calls=%fused_computation.40 | loop fusion | flops 147456 | bytes 393216 | tf_op jit(solution)/shard_map/convert_element_type | solution.py:159
  (43 shorter events, 0.4 us)
Async XLA Ops:
  7.2 59.4 %copy-start = (bf16[1,512,2048]{2,1,0:T(8,128)(2,1)S(1)}, bf16[1,512,2048]{2,1,0:T(8,128)(2,1)}, u32[]{:S(2)}) copy-start(bf16[1,512,2048]{2,1,0:T(8,128)(2,1)} %param.43) | copy-start | bytes 6291460
  7.2 8.4 %copy-start.3 = (bf16[24,2048]{1,0:T(8,128)(2,1)S(1)}, bf16[24,2048]{1,0:T(8,128)(2,1)}, u32[]{:S(2)}) copy-start(bf16[24,2048]{1,0:T(8,128)(2,1)} %param.23) | copy-start | bytes 294916
  7.2 8.4 %copy-start.4 = (bf16[2048,256]{1,0:T(8,128)(2,1)S(1)}, bf16[2048,256]{1,0:T(8,128)(2,1)}, u32[]{:S(2)}) copy-start(bf16[2048,256]{1,0:T(8,128)(2,1)} %param.26) | copy-start | bytes 3145732
  16.0 5.3 %copy-start.1 = (f32[24,2,128,128]{3,2,1,0:T(8,128)S(1)}, f32[24,2,128,128]{3,2,1,0:T(8,128)}, u32[]{:S(2)}) copy-start(f32[24,2,128,128]{3,2,1,0:T(8,128)} %param.24) | copy-start | bytes 9437188
  22.3 1.7 %copy-start.2 = (f32[24,2,128,128]{3,2,1,0:T(8,128)}, f32[24,2,128,128]{3,2,1,0:T(8,128)S(1)}, u32[]{:S(2)}) copy-start(f32[24,2,128,128]{3,2,1,0:T(8,128)S(1)} %multiply_add_fusion) | copy-start | bytes 9437188
  22.4 4.6 %copy-start.5 = (bf16[2048,256]{1,0:T(8,128)(2,1)S(1)}, bf16[2048,256]{1,0:T(8,128)(2,1)}, u32[]{:S(2)}) copy-start(bf16[2048,256]{1,0:T(8,128)(2,1)} %param.29) | copy-start | bytes 3145732
  24.0 3.3 %copy-start.12 = (bf16[128]{0:T(256)(128)(2,1)S(1)}, bf16[128]{0:T(256)(128)(2,1)}, u32[]{:S(2)}) copy-start(bf16[128]{0:T(256)(128)(2,1)} %param.34) | copy-start | bytes 772
  24.0 3.4 %copy-start.6 = (bf16[256,2048]{1,0:T(8,128)(2,1)S(1)}, bf16[256,2048]{1,0:T(8,128)(2,1)}, u32[]{:S(2)}) copy-start(bf16[256,2048]{1,0:T(8,128)(2,1)} %param.35) | copy-start | bytes 3145732
  26.8 11.8 %copy-start.10 = (s32[24,6]{0,1:T(8,128)S(1)}, s32[24,6]{0,1:T(8,128)}, u32[]{:S(2)}) copy-start(s32[24,6]{0,1:T(8,128)} %param.44) | copy-start | bytes 1732
  26.8 12.6 %copy-start.8 = (bf16[2048]{0:T(1024)(128)(2,1)S(1)}, bf16[2048]{0:T(1024)(128)(2,1)}, u32[]{:S(2)}) copy-start(bf16[2048]{0:T(1024)(128)(2,1)} %param.36) | copy-start | bytes 12292
  26.8 12.7 %copy-start.11 = (u32[32]{0:T(128)S(1)}, u32[32]{0:T(128)}, u32[]{:S(2)}) copy-start(u32[32]{0:T(128)} %constant.90) | copy-start | bytes 388
  27.2 27.8 %copy-start.7 = (f32[24,6]{0,1:T(8,128)S(1)}, f32[24,6]{0,1:T(8,128)}, u32[]{:S(2)}) copy-start(f32[24,6]{0,1:T(8,128)} %param.45) | copy-start | bytes 1732
  27.2 27.9 %copy-start.9 = (bf16[2048]{0:T(1024)(128)(2,1)S(1)}, bf16[2048]{0:T(1024)(128)(2,1)}, u32[]{:S(2)}) copy-start(bf16[2048]{0:T(1024)(128)(2,1)} %param.37) | copy-start | bytes 12292
  37.3 3.4 %collective-permute-start = (bf16[6,2048]{1,0:T(8,128)(2,1)S(1)}, bf16[6,2048]{1,0:T(8,128)(2,1)S(1)}, u32[]{:S(2)}, u32[]{:S(2)}) collective-permute-start(bf16[6,2048]{1,0:T(8,128)(2,1)S(1)} %slice.2), channel_id=1, source_target_pairs={{0,1},{1,2},{2,3},{4,5},{5,6},{6,7},{8,9},{9,10},{10,11},{12,13},{... | collective-permute-start | bytes 73736
  49.2 15.3 %all-to-all-start = ((bf16[8,7,2048]{2,1,0:T(8,128)(2,1)}), bf16[8,7,2048]{2,1,0:T(8,128)(2,1)S(1)}, u32[]{:S(2)}, u32[]{:S(2)}) async-start(bf16[8,7,2048]{2,1,0:T(8,128)(2,1)} %reshape.269), calls=%async_computation | async-start | bytes 524288 | tf_op jit(solution)/shard_map/all_to_all | solution.py:143
  69.8 12.6 %all-to-all-start.1 = ((bf16[8,7,2048]{2,1,0:T(8,128)(2,1)}), bf16[8,7,2048]{2,1,0:T(8,128)(2,1)S(1)}, u32[]{:S(2)}, u32[]{:S(2)}) async-start(bf16[8,7,2048]{2,1,0:T(8,128)(2,1)} %reshape.271), calls=%async_computation.1 | async-start | bytes 524288 | tf_op jit(solution)/shard_map/all_to_all | solution.py:147
  73.4 48.1 %all-reduce.4.cloned.1.call-start = ((), (), s32[]{:S(2)}) async-start(), calls=%async_computation.2 | async-start | bytes 196608 | tf_op jit(solution)/shard_map/psum | solution.py:156
Sparse Core Ops, SparseCore 0:
  90.5 30.9 all-reduce.3
where the time goes:
time: 131 us; the launch traced here: 130 us
  waiting for transfers between devices  41.5 us (32%)
  matrix products  24.5 us (19%)
  blocking collectives  22 us (17%)
  between operations  15.1 us (12%)
  starting transfers between devices  10.9 us (8%)
  other arithmetic  8.59 us (7%)
  local copies, waits for them, and re-layouts  7.27 us (6%)
    psum x1, waiting for transfers between devices, shards(): lax.psum((routed_part + blend_gate[:, None] * dense_part).astype(jnp.bflo...  25.7 us
    unnamed x1, blocking collectives  9.66 us
    all_to_all x1, waiting for transfers between devices, shards(): lax.all_to_all(outgoing, 'ep', split_axis=0, concat_axis=0, tiled=True)  9.18 us
    all_gather x1, blocking collectives, shards(): lax.all_gather(normed_rows, 'tp', axis=0, tiled=True)  6.97 us
    all_to_all x1, waiting for transfers between devices, shards(): lax.all_to_all(result.reshape(arrived.shape), 'ep', split_axis=0, concat_...  6.63 us
    all_to_all x1, starting transfers between devices, shards(): lax.all_to_all(outgoing, 'ep', split_axis=0, concat_axis=0, tiled=True)  5.83 us
    all_gather x1, blocking collectives, shards(): lax.all_gather(residual_rows, 'tp', axis=0, tiled=True)  5.42 us
    dot_general x1, matrix products, delta_update(): jnp.einsum('shkv,shk->shv', decayed, key_unit, precision=lax.Precision.HI...  4.94 us
  transfers between devices with their start and end apart: 4, of which 3 were waited for; matrix products, arithmetic and copies ran while one was open for 3% of the time, Pallas kernels for 0%

commit v1 on v0

v1 whole, which is shorter than its diff:
```python
import functools

import jax
import jax.numpy as jnp
from jax import lax
from jax.experimental import pallas as pl
from jax.experimental.pallas import tpu as pltpu
from jax.sharding import PartitionSpec as P

norm_eps = 1e-06
unit_eps = 1e-06
routed_scale = 2.5
vmem_bytes = 60 * 1024 * 1024
MESH = pl.DeviceIdType.MESH
f32 = jnp.float32
bf16 = jnp.bfloat16


def rms_scale(values, gain):
    inverse = lax.rsqrt(jnp.mean(values * values, axis=-1, keepdims=True) + norm_eps)
    return values * inverse * gain


def unit_rows(values):
    return values * lax.rsqrt(jnp.sum(values * values, axis=-1, keepdims=True) + unit_eps)


def silu(values):
    return values * jax.nn.sigmoid(values)


def dot(left, right):
    return jnp.dot(left, right, preferred_element_type=f32)


def mixer_kernel(
    seq_chunk,
    tokens_ref,
    gain_ref,
    head_gain_ref,
    rate_ref,
    bias_ref,
    query_hbm,
    key_hbm,
    value_hbm,
    outgate_hbm,
    beta_hbm,
    decay_hbm,
    out_hbm,
    state_hbm,
    mix_ref,
    new_state_hbm,
    proj_buf,
    beta_buf,
    decay_buf,
    out_buf,
    state_buf,
    column_buf,
    readout_buf,
    proj_sem,
    gate_sem,
    out_sem,
    state_sem,
    store_sem,
):
    seq_count = tokens_ref.shape[0]
    head_local, head_size = state_buf.shape[1:3]
    width = head_local * head_size
    chunk_count = seq_count // seq_chunk
    gate_copies = [
        pltpu.make_async_copy(beta_hbm, beta_buf, gate_sem.at[0]),
        pltpu.make_async_copy(decay_hbm, decay_buf, gate_sem.at[1]),
    ]
    proj_copies = [
        pltpu.make_async_copy(hbm, proj_buf.at[i], proj_sem.at[i])
        for i, hbm in enumerate((key_hbm, query_hbm, value_hbm, outgate_hbm))
    ]
    chunks = [pl.ds(c * seq_chunk, seq_chunk) for c in range(chunk_count)]
    state_copies = [
        pltpu.make_async_copy(state_hbm.at[rows], state_buf.at[rows], state_sem.at[c])
        for c, rows in enumerate(chunks)
    ]
    store_copies = [
        pltpu.make_async_copy(state_buf.at[rows], new_state_hbm.at[rows], store_sem.at[c])
        for c, rows in enumerate(chunks)
    ]
    out_copy = pltpu.make_async_copy(out_hbm, out_buf, out_sem.at[0])
    for copy in proj_copies[:3] + gate_copies + state_copies + proj_copies[3:] + [out_copy]:
        copy.start()

    normed = rms_scale(tokens_ref[...].astype(f32), gain_ref[...].astype(f32)).astype(bf16)

    def project(index):
        proj_copies[index].wait()
        return dot(normed, proj_buf[index]).astype(bf16).astype(f32)

    def heads_of(raw):
        return [raw[:, h * head_size : (h + 1) * head_size] for h in range(head_local)]

    key_units = [unit_rows(silu(raw)) for raw in heads_of(project(0))]
    query_units = [
        unit_rows(silu(raw)) * head_size ** (-0.5) for raw in heads_of(project(1))
    ]
    value_acts = [silu(raw) for raw in heads_of(project(2))]
    for copy in gate_copies:
        copy.wait()
    beta_all = jax.nn.sigmoid(dot(normed, beta_buf[...]))
    decay_all = dot(normed, decay_buf[...])
    lane = lax.broadcasted_iota(jnp.int32, beta_all.shape, 1)
    head_start = lax.axis_index("tp") * head_local
    betas, alphas = [], []
    for h in range(head_local):
        chosen = lane == head_start + h
        betas.append(jnp.sum(jnp.where(chosen, beta_all, 0.0), axis=1, keepdims=True))
        raw = jnp.sum(jnp.where(chosen, decay_all, 0.0), axis=1, keepdims=True)
        raw = raw + bias_ref[head_start + h]
        soft = jnp.maximum(raw, 0.0) + jnp.log1p(jnp.exp(-jnp.abs(raw)))
        alphas.append(jnp.exp(-rate_ref[head_start + h] * soft))
    wide = (seq_count, head_size)
    betas = [jnp.broadcast_to(beta, wide) for beta in betas]
    alphas = [jnp.broadcast_to(alpha, wide) for alpha in alphas]
    stacked = jnp.concatenate(key_units + query_units, axis=0)
    short = -stacked.shape[0] % head_size
    if short:
        stacked = jnp.concatenate([stacked, jnp.zeros((short, head_size), f32)], axis=0)
    column_buf[...] = stacked.T
    for c in range(chunk_count):
        state_copies[c].wait()
        for s in range(c * seq_chunk, (c + 1) * seq_chunk):
            for h in range(head_local):
                key_at = h * seq_count + s
                query_at = (head_local + h) * seq_count + s
                key_column = column_buf[:, key_at : key_at + 1]
                query_column = column_buf[:, query_at : query_at + 1]
                alpha = alphas[h][s : s + 1]
                old = state_buf[s, h]
                predicted = alpha * jnp.sum(old * key_column, axis=0, keepdims=True)
                change = betas[h][s : s + 1] * (value_acts[h][s : s + 1] - predicted)
                new = old * alpha + key_column * change
                state_buf[s, h] = new
                readout_buf[s : s + 1, h * head_size : (h + 1) * head_size] = jnp.sum(
                    new * query_column, axis=0, keepdims=True
                )
        store_copies[c].start()
    outgate = project(3)
    gain = head_gain_ref[...].astype(f32)
    gated = [rms_scale(part, gain) for part in heads_of(readout_buf[...])]
    gated = (jnp.concatenate(gated, axis=1) * silu(outgate)).astype(bf16)
    out_copy.wait()
    half = mix_ref.shape[2]
    for i in range(mix_ref.shape[0]):
        mix_ref[i] = dot(gated, out_buf[:, i * half : (i + 1) * half]).astype(bf16)
    for copy in store_copies:
        copy.wait()


def expert_kernel(
    ep_count,
    tp_count,
    capacity,
    mix_ref,
    tokens_ref,
    gain_ref,
    blend_ref,
    ids_ref,
    weights_ref,
    dense_gate_hbm,
    dense_up_hbm,
    dense_down_hbm,
    gate_hbm,
    up_hbm,
    down_hbm,
    out_ref,
    wide_buf,
    dense_down_buf,
    down_buf,
    pair_buf,
    chip_buf,
    cross_buf,
    residual_buf,
    part_buf,
    pair_two_buf,
    chip_two_buf,
    cross_two_buf,
    final_buf,
    outgoing_buf,
    arrived_buf,
    result_buf,
    returned_buf,
    rows_buf,
    weight_sem,
    tp_send,
    tp_recv,
    ep_send,
    ep_recv,
):
    seq_count, width = tokens_ref.shape
    half = width // 2
    slot_rows = outgoing_buf.shape[1]
    me = lax.axis_index("ep")
    tp_index = lax.axis_index("tp")
    core = lax.rem(tp_index, 2)
    chip = tp_index // 2
    partner = chip * 2 + 1 - core
    across = lax.rem(chip + 1, 2) * 2 + core

    weight_copies = [
        pltpu.make_async_copy(hbm, buf, weight_sem.at[i])
        for i, (hbm, buf) in enumerate(
            (
                (dense_gate_hbm, wide_buf.at[0]),
                (dense_up_hbm, wide_buf.at[1]),
                (dense_down_hbm, dense_down_buf),
                (gate_hbm.at[0], wide_buf.at[2]),
                (up_hbm.at[0], wide_buf.at[3]),
                (down_hbm.at[0], down_buf),
            )
        )
    ]
    barrier = pltpu.get_barrier_semaphore()
    pl.semaphore_signal(barrier, inc=1, device_id={"tp": partner}, device_id_type=MESH)
    pl.semaphore_signal(barrier, inc=1, device_id={"tp": across}, device_id_type=MESH)

    def greet(step, carry):
        peer = lax.rem(me + step, ep_count)
        pl.semaphore_signal(barrier, inc=1, device_id={"ep": peer}, device_id_type=MESH)
        return carry

    lax.fori_loop(1, ep_count, greet, 0)
    for copy in weight_copies:
        copy.start()
    pl.semaphore_wait(barrier, ep_count + 1)

    def tp_copy(src, dst, index, target):
        return pltpu.make_async_remote_copy(
            src_ref=src,
            dst_ref=dst,
            send_sem=tp_send.at[index],
            recv_sem=tp_recv.at[index],
            device_id={"tp": target},
            device_id_type=MESH,
        )

    def start_pair(source, pair, base):
        copy = tp_copy(source.at[1 - core], pair, base, partner)
        copy.start()
        return copy

    def finish_sum(copy, source, pair, chip_sum, cross, base):
        copy.wait()
        chip_sum[...] = (source[core].astype(f32) + pair[...].astype(f32)).astype(bf16)
        other = tp_copy(chip_sum, cross, base + 1, across)
        other.start()
        other.wait()
        return chip_sum[...].astype(f32) + cross[...].astype(f32)

    def share(buf, base):
        copy = tp_copy(buf.at[core], buf.at[core], base + 2, partner)
        copy.start()
        tp_copy(buf.at[1 - core], buf.at[1 - core], base + 2, partner).wait_recv()
        copy.wait_send()

    first = start_pair(mix_ref, pair_buf, 0)

    expert_count = ep_count * tp_count
    slot_total = ep_count * slot_rows
    ids = ids_ref[...]
    raw_weights = weights_ref[...]
    scales = raw_weights / jnp.sum(raw_weights, axis=1, keepdims=True) * routed_scale
    expert_lane = lax.broadcasted_iota(jnp.int32, (seq_count, slot_total), 1)
    slot_expert = expert_lane // slot_rows * tp_count + tp_index
    slot_place = lax.rem(expert_lane, slot_rows)
    named = jnp.zeros((seq_count, slot_total), f32)
    scale_at = jnp.zeros((seq_count, slot_total), f32)
    for k in range(ids.shape[1]):
        same = ids[:, k : k + 1] == slot_expert
        named = named + jnp.where(same, 1.0, 0.0)
        scale_at = scale_at + jnp.where(same, scales[:, k : k + 1], 0.0)
    row = lax.broadcasted_iota(jnp.int32, (seq_count, seq_count), 0)
    col = lax.broadcasted_iota(jnp.int32, (seq_count, seq_count), 1)
    earlier = jnp.where(row > col, 1.0, 0.0).astype(bf16)
    rank = dot(earlier, named.astype(bf16))
    taken = named * jnp.where(rank == slot_place.astype(f32), 1.0, 0.0)
    scale_at = scale_at * taken
    scale_high = scale_at.astype(bf16)
    scale_low = (scale_at - scale_high.astype(f32)).astype(bf16)
    dispatch = taken.astype(bf16)

    mixed = finish_sum(first, mix_ref, pair_buf, chip_buf, cross_buf, 0)
    own_tokens = jnp.where(core == 0, tokens_ref[:, :half].astype(f32), tokens_ref[:, half:].astype(f32))
    residual_buf[core] = (own_tokens + mixed).astype(bf16)
    share(residual_buf, 0)
    residual = jnp.concatenate([residual_buf[0], residual_buf[1]], axis=1).astype(f32)
    normed = rms_scale(residual, gain_ref[...].astype(f32)).astype(bf16)
    outgoing = lax.dot_general(
        dispatch, normed, (((0,), (0,)), ((), ())), preferred_element_type=f32
    )
    rows_buf[...] = outgoing

    def fill(peer, carry):
        block = rows_buf[pl.ds(pl.multiple_of(peer * slot_rows, slot_rows), slot_rows), :]
        outgoing_buf[peer] = block.astype(bf16)
        return carry

    lax.fori_loop(0, ep_count, fill, 0, unroll=ep_count <= 8)

    def ep_copy(src, dst, index, src_at, dst_at, target):
        return pltpu.make_async_remote_copy(
            src_ref=src.at[src_at],
            dst_ref=dst.at[dst_at],
            send_sem=ep_send.at[index, src_at],
            recv_sem=ep_recv.at[index, dst_at],
            device_id={"ep": target},
            device_id_type=MESH,
        )

    def send_all(src, dst, index):
        def step_of(step, carry):
            peer = lax.rem(me + step, ep_count)
            ep_copy(src, dst, index, peer, me, peer).start()
            return carry

        lax.fori_loop(1, ep_count, step_of, 0, unroll=ep_count <= 8)
        dst[me] = src[me]

    def wait_all(src, dst, index):
        def step_of(step, carry):
            peer = lax.rem(me + step, ep_count)
            ep_copy(src, dst, index, peer, peer, peer).wait()
            return carry

        lax.fori_loop(1, ep_count, step_of, 0, unroll=ep_count <= 8)

    def gather_rows(buf):
        def step_of(peer, carry):
            at = pl.ds(pl.multiple_of(peer * slot_rows, slot_rows), slot_rows)
            rows_buf[at, :] = buf[peer].astype(f32)
            return carry

        lax.fori_loop(0, ep_count, step_of, 0, unroll=ep_count <= 8)
        return rows_buf[...].astype(bf16)

    send_all(outgoing_buf, arrived_buf, 0)

    blend_row = blend_ref[...].astype(f32)
    blend_gate = jax.nn.sigmoid(
        jnp.sum(normed.astype(f32) * blend_row, axis=1, keepdims=True)
    )
    weight_copies[0].wait()
    dense_gate = dot(normed, wide_buf[0])
    weight_copies[1].wait()
    dense_hidden = (silu(dense_gate) * dot(normed, wide_buf[1])).astype(bf16)
    weight_copies[2].wait()
    dense_part = blend_gate * dot(dense_hidden, dense_down_buf[...])

    wait_all(outgoing_buf, arrived_buf, 0)
    rows = gather_rows(arrived_buf)
    weight_copies[3].wait()
    gate_part = dot(rows, wide_buf[2])
    weight_copies[4].wait()
    hidden = (silu(gate_part) * dot(rows, wide_buf[3])).astype(bf16)
    weight_copies[5].wait()
    rows_buf[...] = dot(hidden, down_buf[...])

    def fill_result(peer, carry):
        block = rows_buf[pl.ds(pl.multiple_of(peer * slot_rows, slot_rows), slot_rows), :]
        result_buf[peer] = block.astype(bf16)
        return carry

    lax.fori_loop(0, ep_count, fill_result, 0, unroll=ep_count <= 8)
    send_all(result_buf, returned_buf, 1)
    wait_all(result_buf, returned_buf, 1)
    rows = gather_rows(returned_buf)
    total = dense_part + dot(scale_high, rows) + dot(scale_low, rows)
    part_buf[0] = total[:, :half].astype(bf16)
    part_buf[1] = total[:, half:].astype(bf16)
    second = start_pair(part_buf, pair_two_buf, 3)
    combined = finish_sum(second, part_buf, pair_two_buf, chip_two_buf, cross_two_buf, 3)
    final_buf[core] = (residual_buf[core].astype(f32) + combined).astype(bf16)
    share(final_buf, 3)
    out_ref[:, :half] = final_buf[0]
    out_ref[:, half:] = final_buf[1]


def shards(
    tokens,
    delta_state,
    first_gain,
    query_weight,
    key_weight,
    value_weight,
    outgate_weight,
    beta_weight,
    decay_weight,
    decay_rate,
    decay_bias,
    head_gain,
    out_weight,
    second_gain,
    blend_weight,
    dense_gate_weight,
    dense_up_weight,
    dense_down_weight,
    expert_gate,
    expert_up,
    expert_down,
    route_ids,
    route_weights,
):
    seq_count, width = tokens.shape
    head_local, head_size = delta_state.shape[1:3]
    ep_count = lax.axis_size("ep")
    tp_count = lax.axis_size("tp")
    half = width // 2
    vmem = pl.BlockSpec(memory_space=pltpu.VMEM)
    smem = pl.BlockSpec(memory_space=pltpu.SMEM)
    hbm = pl.BlockSpec(memory_space=pl.ANY)
    dma = pltpu.SemaphoreType.DMA
    seq_chunk = 4 if seq_count % 4 == 0 else 1
    local_width = query_weight.shape[1]
    stacked = -(-2 * head_local * seq_count // head_size) * head_size
    mix_part, new_state = pl.pallas_call(
        functools.partial(mixer_kernel, seq_chunk),
        out_shape=(
            jax.ShapeDtypeStruct((2, seq_count, half), bf16),
            jax.ShapeDtypeStruct(delta_state.shape, f32),
        ),
        in_specs=[vmem] * 3 + [smem] * 2 + [hbm] * 8,
        out_specs=(vmem, hbm),
        scratch_shapes=[
            pltpu.VMEM((4,) + query_weight.shape, bf16),
            pltpu.VMEM(beta_weight.shape, bf16),
            pltpu.VMEM(decay_weight.shape, bf16),
            pltpu.VMEM(out_weight.shape, bf16),
            pltpu.VMEM(delta_state.shape, f32),
            pltpu.VMEM((head_size, stacked), f32),
            pltpu.VMEM((seq_count, local_width), f32),
            dma((4,)),
            dma((2,)),
            dma((1,)),
            dma((seq_count // seq_chunk,)),
            dma((seq_count // seq_chunk,)),
        ],
        compiler_params=pltpu.CompilerParams(vmem_limit_bytes=vmem_bytes),
        name="mixer",
    )(
        tokens,
        first_gain.reshape(1, -1),
        head_gain.reshape(1, -1),
        decay_rate,
        decay_bias,
        query_weight,
        key_weight,
        value_weight,
        outgate_weight,
        beta_weight,
        decay_weight,
        out_weight,
        delta_state,
    )
    top_count = route_ids.shape[1]
    expert_count = ep_count * tp_count
    capacity = max(2, (3 * seq_count * top_count + 2 * expert_count - 1) // (2 * expert_count))
    slot_rows = -(-capacity // 8) * 8
    wide = pltpu.VMEM((4,) + dense_gate_weight.shape, bf16)
    half_block = pltpu.VMEM((seq_count, half), bf16)
    both_block = pltpu.VMEM((2, seq_count, half), bf16)
    slots = pltpu.VMEM((ep_count, slot_rows, width), bf16)
    new_tokens = pl.pallas_call(
        functools.partial(expert_kernel, ep_count, tp_count, capacity),
        out_shape=jax.ShapeDtypeStruct(tokens.shape, bf16),
        in_specs=[vmem] * 6 + [hbm] * 6,
        out_specs=vmem,
        scratch_shapes=[
            wide,
            pltpu.VMEM(dense_down_weight.shape, bf16),
            pltpu.VMEM(expert_down.shape[1:], bf16),
            half_block,
            half_block,
            half_block,
            both_block,
            both_block,
            half_block,
            half_block,
            half_block,
            both_block,
            slots,
            slots,
            slots,
            slots,
            pltpu.VMEM((ep_count * slot_rows, width), f32),
            dma((6,)),
            dma((6,)),
            dma((6,)),
            dma((2, ep_count)),
            dma((2, ep_count)),
        ],
        compiler_params=pltpu.CompilerParams(
            vmem_limit_bytes=vmem_bytes, collective_id=0, has_side_effects=True
        ),
        name="experts",
    )(
        mix_part,
        tokens,
        second_gain.reshape(1, -1),
        blend_weight.reshape(1, -1),
        route_ids,
        route_weights,
        dense_gate_weight,
        dense_up_weight,
        dense_down_weight,
        expert_gate,
        expert_up,
        expert_down,
    )
    return (new_tokens, new_state)


def solution(mesh):
    placed = (
        P("ep", None),
        P("ep", "tp", None, None),
        P(),
        P(None, "tp"),
        P(None, "tp"),
        P(None, "tp"),
        P(None, "tp"),
        P(),
        P(),
        P(),
        P(),
        P(),
        P("tp", None),
        P(),
        P(),
        P(None, "tp"),
        P(None, "tp"),
        P("tp", None),
        P(("ep", "tp"), None, None),
        P(("ep", "tp"), None, None),
        P(("ep", "tp"), None, None),
        P("ep", None),
        P("ep", None),
    )
    return jax.shard_map(
        shards,
        mesh=mesh,
        in_specs=placed,
        out_specs=(P("ep", None), P("ep", "tp", None, None)),
        check_vma=False,
    )
```

time: 131 us -> 51.4 us (0.39)
  waiting for transfers between devices: 41.5 us -> 0 us
  Pallas kernels: 0 us -> 41.4 us
  matrix products: 24.5 us -> 0 us
  blocking collectives: 22 us -> 0 us
  between operations: 15.1 us -> 0.66 us
  starting transfers between devices: 10.9 us -> 0 us
  other arithmetic: 8.59 us -> 0 us
  local copies, waits for them, and re-layouts: 7.27 us -> 8.94 us
    pallas_call x0 -> x2, Pallas kernels: none -> 41.4 us  [the longest x1 33.1 us: shards(): pl.pallas_call(functools.partial(expert_kernel, ep_count, tp_count, capac...]
    psum x1 -> x0, waiting for transfers between devices: 25.7 us -> none  [shards(): lax.psum((routed_part + blend_gate[:, None] * dense_part).astype(jnp.bflo...]
    dot_general x15 -> x0, matrix products: 24.5 us -> none  [the longest x1 4.94 us: delta_update(): jnp.einsum('shkv,shk->shv', decayed, key_unit, precision=lax.Precision.HI...]
    all_to_all x2 -> x0, waiting for transfers between devices: 15.8 us -> none  [the longest x1 9.18 us: shards(): lax.all_to_all(outgoing, 'ep', split_axis=0, concat_axis=0, tiled=True)]
    all_gather x2 -> x0, blocking collectives: 12.4 us -> none  [the longest x1 6.97 us: shards(): lax.all_gather(normed_rows, 'tp', axis=0, tiled=True)]
    unnamed x1 -> x0, blocking collectives: 9.66 us -> none
    all_to_all x2 -> x0, starting transfers between devices: 9.42 us -> none  [the longest x1 5.83 us: shards(): lax.all_to_all(outgoing, 'ep', split_axis=0, concat_axis=0, tiled=True)]
    unnamed x33 -> x13, local copies, waits for them, and re-layouts: 2.58 us -> 6.45 us
  transfers between devices with their start and end apart: 4 -> 0, of which waited for: 3 -> 0; matrix products, arithmetic and copies ran while one was open for 3% -> 0% of each run, Pallas kernels for 0% -> 0%
where the time goes in v1:
time: 51.4 us; the launch traced here: 51 us
  Pallas kernels  41.4 us (81%)
  local copies, waits for them, and re-layouts  8.94 us (17%)
  between operations  0.66 us (1%)
    pallas_call x1, Pallas kernels, shards(): pl.pallas_call(functools.partial(expert_kernel, ep_count, tp_count, capac...  33.1 us
    pallas_call x1, Pallas kernels, shards(): pl.pallas_call(functools.partial(mixer_kernel, seq_chunk), out_shape=(jax...  8.29 us
    unnamed x13, local copies, waits for them, and re-layouts  6.45 us
    reshape x1, local copies, waits for them, and re-layouts, shards(): first_gain.reshape(1, -1)  1.29 us

profile of v1, /device:TPU:0, one launch (start us, length us, event | category | flops | bytes accessed | tf_op | source)
XLA Modules:
  0.0 51.0 jit_solution(6732622816675999607)
XLA Ops:
  0.6 1.8 %copy.25.beta_hbm = bf16[2048,8]{1,0:T(8,128)(2,1)} copy(bf16[2048,8]{0,1:T(8,128)(2,1)} %param.30) | data formatting | bytes 65536 | tf_op args[7]
  2.4 1.8 %copy.26.decay_hbm = bf16[2048,8]{1,0:T(8,128)(2,1)} copy(bf16[2048,8]{0,1:T(8,128)(2,1)} %param.31) | data formatting | bytes 65536 | tf_op args[8]
  4.2 1.3 %reshape.16.gain_ref = bf16[1,2048]{1,0:T(2,128)(2,1)} reshape(bf16[2048]{0:T(1024)(128)(2,1)} %param.25) | data formatting | bytes 8192 | tf_op jit(solution)/shard_map/reshape | solution.py:448
  5.4 0.0 copy-start.2
  5.4 0.0 copy-start.3
  5.5 0.0 copy-start
  5.5 0.0 copy-start.1
  5.5 8.3 %mixer.1 = (bf16[2,24,1024]{2,1,0:T(8,128)(2,1)}, f32[24,2,128,128]{3,2,1,0:T(8,128)}) custom-call(bf16[24,2048]{1,0:T(8,128)(2,1)} %tokens_ref.3, bf16[1,2048]{1,0:T(2,128)(2,1)} %reshape.16.gain_ref, bf16[1,128]{1,0:T(2,128)(2,1)} %bitcast.1, f32[8]{0:T(128)} %rate_ref.1, f32[8]{0:T(128)} %bias_ref.1, bf16[2048,256]{1,0:T(8,128)(2,1)} %query_hbm.1, ...), custom_call_target="tpu_custom_call" | custom-call | tf_op jit(solution)/shard_map/mixer/pallas_call | solution.py:422
  13.8 0.0 copy-done.2
  13.8 0.7 %copy.27.ids_ref = s32[24,6]{1,0:T(8,128)} copy(s32[24,6]{0,1:T(8,128)S(1)} %copy-done.2) | data formatting | bytes 1152 | tf_op args[21]
  14.5 0.0 copy-done.3
  14.5 0.7 %copy.28.weights_ref = f32[24,6]{1,0:T(8,128)} copy(f32[24,6]{0,1:T(8,128)S(1)} %copy-done.3) | data formatting | bytes 1152 | tf_op args[22]
  15.1 0.0 copy-done
  15.1 0.6 %reshape.18.gain_ref = bf16[1,2048]{1,0:T(2,128)(2,1)} reshape(bf16[2048]{0:T(1024)(128)(2,1)S(1)} %copy-done) | data formatting | bytes 8192 | tf_op jit(solution)/shard_map/reshape | solution.py:505
  15.7 0.0 copy-done.1
  15.7 0.6 %reshape.19.blend_ref = bf16[1,2048]{1,0:T(2,128)(2,1)} reshape(bf16[2048]{0:T(1024)(128)(2,1)S(1)} %copy-done.1) | data formatting | bytes 8192 | tf_op jit(solution)/shard_map/reshape | solution.py:506
  16.3 33.1 %experts.1 = bf16[24,2048]{1,0:T(8,128)(2,1)} custom-call(bf16[2,24,1024]{2,1,0:T(8,128)(2,1)} %get-tuple-element.4.mix_ref, bf16[24,2048]{1,0:T(8,128)(2,1)} %tokens_ref.3, bf16[1,2048]{1,0:T(2,128)(2,1)} %reshape.18.gain_ref, bf16[1,2048]{1,0:T(2,128)(2,1)} %reshape.19.blend_ref, s32[24,6]{1,0:T(8,128)} %copy.27.ids_ref, f32[24,6]{1,0:T(8,128)} %copy.28.weights_ref, ...), custom_call_target="tpu_custom_call" | custom-call | tf_op jit(solution)/shard_map/experts/pallas_call | solution.py:469
  49.4 1.5 %copy.30 = bf16[24,2048]{1,0:T(8,128)(2,1)} copy(bf16[24,2048]{1,0:T(8,128)(2,1)} %experts.1) | data formatting | bytes 196608
Async XLA Ops:
  5.4 8.3 %copy-start.2 = (s32[24,6]{0,1:T(8,128)S(1)}, s32[24,6]{0,1:T(8,128)}, u32[]{:S(2)}) copy-start(s32[24,6]{0,1:T(8,128)} %param.44) | copy-start | bytes 1732
  5.4 9.0 %copy-start.3 = (f32[24,6]{0,1:T(8,128)S(1)}, f32[24,6]{0,1:T(8,128)}, u32[]{:S(2)}) copy-start(f32[24,6]{0,1:T(8,128)} %param.45) | copy-start | bytes 1732
  5.5 9.7 %copy-start = (bf16[2048]{0:T(1024)(128)(2,1)S(1)}, bf16[2048]{0:T(1024)(128)(2,1)}, u32[]{:S(2)}) copy-start(bf16[2048]{0:T(1024)(128)(2,1)} %param.36) | copy-start | bytes 12292
  5.5 10.3 %copy-start.1 = (bf16[2048]{0:T(1024)(128)(2,1)S(1)}, bf16[2048]{0:T(1024)(128)(2,1)}, u32[]{:S(2)}) copy-start(bf16[2048]{0:T(1024)(128)(2,1)} %param.37) | copy-start | bytes 12292

commit v2 on v1

--- a/solution.py
+++ b/solution.py
@@ -31,6 +31,14 @@
 
 def dot(left, right):
     return jnp.dot(left, right, preferred_element_type=f32)
+
+
+def dot_t(left, right):
+    return lax.dot_general(left, right, (((1,), (1,)), ((), ())), preferred_element_type=f32)
+
+
+def row_of(ref):
+    return ref[...].astype(f32).reshape(1, -1)
 
 
 def mixer_kernel(
@@ -88,7 +96,7 @@
     for copy in proj_copies[:3] + gate_copies + state_copies + proj_copies[3:] + [out_copy]:
         copy.start()
 
-    normed = rms_scale(tokens_ref[...].astype(f32), gain_ref[...].astype(f32)).astype(bf16)
+    normed = rms_scale(tokens_ref[...].astype(f32), row_of(gain_ref)).astype(bf16)
 
     def project(index):
         proj_copies[index].wait()
@@ -104,8 +112,8 @@
     value_acts = [silu(raw) for raw in heads_of(project(2))]
     for copy in gate_copies:
         copy.wait()
-    beta_all = jax.nn.sigmoid(dot(normed, beta_buf[...]))
-    decay_all = dot(normed, decay_buf[...])
+    beta_all = jax.nn.sigmoid(dot_t(normed, beta_buf[...]))
+    decay_all = dot_t(normed, decay_buf[...])
     lane = lax.broadcasted_iota(jnp.int32, beta_all.shape, 1)
     head_start = lax.axis_index("tp") * head_local
     betas, alphas = [], []
@@ -143,7 +151,7 @@
                 )
         store_copies[c].start()
     outgate = project(3)
-    gain = head_gain_ref[...].astype(f32)
+    gain = row_of(head_gain_ref)
     gated = [rms_scale(part, gain) for part in heads_of(readout_buf[...])]
     gated = (jnp.concatenate(gated, axis=1) * silu(outgate)).astype(bf16)
     out_copy.wait()
@@ -266,22 +274,22 @@
     slot_total = ep_count * slot_rows
     ids = ids_ref[...]
     raw_weights = weights_ref[...]
-    scales = raw_weights / jnp.sum(raw_weights, axis=1, keepdims=True) * routed_scale
-    expert_lane = lax.broadcasted_iota(jnp.int32, (seq_count, slot_total), 1)
-    slot_expert = expert_lane // slot_rows * tp_count + tp_index
-    slot_place = lax.rem(expert_lane, slot_rows)
-    named = jnp.zeros((seq_count, slot_total), f32)
-    scale_at = jnp.zeros((seq_count, slot_total), f32)
-    for k in range(ids.shape[1]):
-        same = ids[:, k : k + 1] == slot_expert
+    scales = raw_weights / jnp.sum(raw_weights, axis=0, keepdims=True) * routed_scale
+    slot = lax.broadcasted_iota(jnp.int32, (slot_total, seq_count), 0)
+    slot_expert = slot // slot_rows * tp_count + tp_index
+    slot_place = lax.rem(slot, slot_rows)
+    named = jnp.zeros((slot_total, seq_count), f32)
+    scale_at = jnp.zeros((slot_total, seq_count), f32)
+    for k in range(ids.shape[0]):
+        same = ids[k : k + 1] == slot_expert
         named = named + jnp.where(same, 1.0, 0.0)
-        scale_at = scale_at + jnp.where(same, scales[:, k : k + 1], 0.0)
+        scale_at = scale_at + jnp.where(same, scales[k : k + 1], 0.0)
     row = lax.broadcasted_iota(jnp.int32, (seq_count, seq_count), 0)
     col = lax.broadcasted_iota(jnp.int32, (seq_count, seq_count), 1)
-    earlier = jnp.where(row > col, 1.0, 0.0).astype(bf16)
-    rank = dot(earlier, named.astype(bf16))
+    earlier = jnp.where(row < col, 1.0, 0.0).astype(bf16)
+    rank = dot(named.astype(bf16), earlier)
     taken = named * jnp.where(rank == slot_place.astype(f32), 1.0, 0.0)
-    scale_at = scale_at * taken
+    scale_at = (scale_at * taken).T
     scale_high = scale_at.astype(bf16)
     scale_low = (scale_at - scale_high.astype(f32)).astype(bf16)
     dispatch = taken.astype(bf16)
@@ -291,11 +299,8 @@
     residual_buf[core] = (own_tokens + mixed).astype(bf16)
     share(residual_buf, 0)
     residual = jnp.concatenate([residual_buf[0], residual_buf[1]], axis=1).astype(f32)
-    normed = rms_scale(residual, gain_ref[...].astype(f32)).astype(bf16)
-    outgoing = lax.dot_general(
-        dispatch, normed, (((0,), (0,)), ((), ())), preferred_element_type=f32
-    )
-    rows_buf[...] = outgoing
+    normed = rms_scale(residual, row_of(gain_ref)).astype(bf16)
+    rows_buf[...] = dot(dispatch, normed)
 
     def fill(peer, carry):
         block = rows_buf[pl.ds(pl.multiple_of(peer * slot_rows, slot_rows), slot_rows), :]
@@ -342,7 +347,7 @@
 
     send_all(outgoing_buf, arrived_buf, 0)
 
-    blend_row = blend_ref[...].astype(f32)
+    blend_row = row_of(blend_ref)
     blend_gate = jax.nn.sigmoid(
         jnp.sum(normed.astype(f32) * blend_row, axis=1, keepdims=True)
     )
@@ -429,8 +434,8 @@
         out_specs=(vmem, hbm),
         scratch_shapes=[
             pltpu.VMEM((4,) + query_weight.shape, bf16),
-            pltpu.VMEM(beta_weight.shape, bf16),
-            pltpu.VMEM(decay_weight.shape, bf16),
+            pltpu.VMEM(beta_weight.shape[::-1], bf16),
+            pltpu.VMEM(decay_weight.shape[::-1], bf16),
             pltpu.VMEM(out_weight.shape, bf16),
             pltpu.VMEM(delta_state.shape, f32),
             pltpu.VMEM((head_size, stacked), f32),
@@ -445,16 +450,16 @@
         name="mixer",
     )(
         tokens,
-        first_gain.reshape(1, -1),
-        head_gain.reshape(1, -1),
+        first_gain,
+        head_gain,
         decay_rate,
         decay_bias,
         query_weight,
         key_weight,
         value_weight,
         outgate_weight,
-        beta_weight,
-        decay_weight,
+        beta_weight.T,
+        decay_weight.T,
         out_weight,
         delta_state,
     )
@@ -502,10 +507,10 @@
     )(
         mix_part,
         tokens,
-        second_gain.reshape(1, -1),
-        blend_weight.reshape(1, -1),
-        route_ids,
-        route_weights,
+        second_gain,
+        blend_weight,
+        route_ids.T,
+        route_weights.T,
         dense_gate_weight,
         dense_up_weight,
         dense_down_weight,

time: 51.4 us -> 43.6 us (0.85)
  local copies, waits for them, and re-layouts: 8.94 us -> 1.54 us
    unnamed x13 -> x1, local copies, waits for them, and re-layouts: 6.45 us -> 1.54 us
    reshape x3 -> x0, local copies, waits for them, and re-layouts: 2.49 us -> none  [the longest x1 1.29 us: shards(): first_gain.reshape(1, -1)]
where the time goes in v2:
time: 43.6 us; the launch traced here: 43.4 us
  Pallas kernels  41.2 us (94%)
  local copies, waits for them, and re-layouts  1.54 us (4%)
  between operations  0.65 us (1%)
    pallas_call x1, Pallas kernels, shards(): pl.pallas_call(functools.partial(expert_kernel, ep_count, tp_count, capac...  33.1 us
    pallas_call x1, Pallas kernels, shards(): pl.pallas_call(functools.partial(mixer_kernel, seq_chunk), out_shape=(jax...  8.09 us
    unnamed x1, local copies, waits for them, and re-layouts  1.54 us

profile of v2, /device:TPU:0, one launch (start us, length us, event | category | flops | bytes accessed | tf_op | source)
XLA Modules:
  0.0 43.4 jit_solution(9965427931117154056)
XLA Ops:
  0.6 8.1 %mixer.1 = (bf16[2,24,1024]{2,1,0:T(8,128)(2,1)}, f32[24,2,128,128]{3,2,1,0:T(8,128)}) custom-call(bf16[24,2048]{1,0:T(8,128)(2,1)} %tokens_ref.3, bf16[2048]{0:T(1024)(128)(2,1)} %gain_ref.2, bf16[128]{0:T(256)(128)(2,1)} %head_gain_ref.1, f32[8]{0:T(128)} %rate_ref.1, f32[8]{0:T(128)} %bias_ref.1, bf16[2048,256]{1,0:T(8,128)(2,1)} %query_hbm.1, ...), custom_call_target="tpu_custom_call" | custom-call | tf_op jit(solution)/shard_map/mixer/pallas_call | solution.py:427
  8.7 33.1 %experts.1 = bf16[24,2048]{1,0:T(8,128)(2,1)} custom-call(bf16[2,24,1024]{2,1,0:T(8,128)(2,1)} %get-tuple-element.4.mix_ref, bf16[24,2048]{1,0:T(8,128)(2,1)} %tokens_ref.3, bf16[2048]{0:T(1024)(128)(2,1)} %gain_ref.3, bf16[2048]{0:T(1024)(128)(2,1)} %blend_ref.1, s32[6,24]{1,0:T(8,128)} %bitcast.6, f32[6,24]{1,0:T(8,128)} %bitcast.7, ...), custom_call_target="tpu_custom_call" | custom-call | tf_op jit(solution)/shard_map/experts/pallas_call | solution.py:474
  41.8 1.5 %copy.26 = bf16[24,2048]{1,0:T(8,128)(2,1)} copy(bf16[24,2048]{1,0:T(8,128)(2,1)} %experts.1) | data formatting | bytes 196608
